TPU v7x, 32 devices: a whole 2x2x4 slice. The times are simulated.
32 devices in a mesh: kv: 8 (over z, y), tp: 4 (over x, core).
Axes of the slice: x: 2, y: 2, z: 4, core: 2. Of those that a mesh axis runs over, the one named last changes fastest.
Arguments:
- tokens: bfloat16 [16, 4096], P(None, ('kv', 'tp')), may hold values from -17 to 17
- first_gain: float32 [4096], P('kv'), may hold values from 0.1 to 1.9
- first_gate: bfloat16 [4096, 11264], P('kv', 'tp'), may hold values from -0.09375 to 0.09375
- first_up: bfloat16 [4096, 11264], P('kv', 'tp'), may hold values from -0.09375 to 0.09375
- first_down: bfloat16 [11264, 4096], P('tp', 'kv'), may hold values from -0.0546875 to 0.0546875
- mixer_gain: float32 [4096], P('kv'), may hold values from 0.1 to 1.9
- w_query: bfloat16 [4096, 4096], P('kv', 'tp'), may hold values from -0.09375 to 0.09375
- w_key: bfloat16 [4096, 4096], P('kv', 'tp'), may hold values from -0.328125 to 0.328125
- w_value: bfloat16 [4096, 4096], P('kv', 'tp'), may hold values from -0.09375 to 0.09375
- w_output: bfloat16 [4096, 4096], P('tp', 'kv'), may hold values from -0.09375 to 0.09375
- lam_heads: float32 [32], P('tp'), may hold values from 0.3 to 0.8
- head_gain: float32 [128], replicated, may hold values from 0.1 to 1.9
- key_cache: bfloat16 [16, 2048, 32, 128], P(None, 'kv', 'tp'), may hold values from -1000 to 1000
- value_cache: bfloat16 [16, 2048, 32, 128], P(None, 'kv', 'tp'), may hold values from -6 to 6
- lengths: int32 [16], replicated, may hold values from 1 to 2048, 12288 in all
- last_gain: float32 [4096], P('kv'), may hold values from 0.1 to 1.9
- last_gate: bfloat16 [4096, 11264], P('kv', 'tp'), may hold values from -0.09375 to 0.09375
- last_up: bfloat16 [4096, 11264], P('kv', 'tp'), may hold values from -0.09375 to 0.09375
- last_down: bfloat16 [11264, 4096], P('tp', 'kv'), may hold values from -0.0546875 to 0.0546875
Outputs:
- result: bfloat16 [16, 4096], P(None, ('kv', 'tp'))
Inputs may be any that keep to these rules, and one draw needn't show every extreme that they name: Sequence b reads cached positions 0 to lengths[b] - 1 and its new token.
All inputs are finite; a program needn't handle non-finite values.
Results may differ from a plain program's by a relative error of at most 0.04.
Values may be sent and summed in bfloat16 or wider, within the bound.
A program may use at most 128 MiB of HBM per device.

v0:
```python
import functools

import jax
import jax.numpy as jnp
from jax import lax
from jax.experimental import pallas as pl
from jax.experimental.pallas import tpu as pltpu
from jax.sharding import PartitionSpec as P

HEAD_DIM = 64
VAL_DIM = 128
LANE = 128
epsilon = 1e-06
neg_fill = -1e30
bf16 = jnp.bfloat16
f32 = jnp.float32
MESH = pl.DeviceIdType.MESH


def ceil_div(a, b):
    return -(-a // b)


def layer_kernel(
    cfg,
    tokens,
    first_gain,
    mixer_gain,
    last_gain,
    head_gain,
    lam,
    lengths,
    first_gate,
    first_up,
    first_down,
    w_query,
    w_key,
    w_value,
    w_output,
    keys,
    values,
    last_gate,
    last_up,
    last_down,
    result,
    g1,
    u1,
    d1,
    wq,
    wk,
    wv,
    wo,
    kc,
    vc,
    g2,
    u2,
    d2,
    tok_all,
    stream,
    gu_send1,
    gu_recv1,
    gu_send2,
    gu_recv2,
    hid1,
    hid2,
    down1,
    down2,
    down2_recv,
    qkv_send,
    qkv_recv,
    q_all,
    qf,
    acc,
    pos_ref,
    att_send,
    att_recv,
    att_all,
    out_all,
    load_sem,
    send_sem,
    tok_sem,
    gu_sem1,
    gu_sem2,
    hid_sem1,
    hid_sem2,
    down_sem1,
    down_sem2,
    qkv_sem,
    q_sem,
    part_sem,
    att_sem,
    out_sem,
):
    n, t, width, rows = cfg["n"], cfg["t"], cfg["width"], cfg["rows"]
    heads, positions = cfg["heads"], cfg["positions"]
    units, span, own_heads = cfg["units"], cfg["span"], cfg["own_heads"]
    cols, gather_here = cfg["cols"], cfg["gather_here"]
    head_span = own_heads * VAL_DIM
    inner = heads * VAL_DIM
    me_k = lax.axis_index("kv")
    me_t = lax.axis_index("tp")

    def load(source, target, index):
        return pltpu.make_async_copy(source, target, load_sem.at[index])

    def padded(ref, axis, size):
        if ref.shape[axis] == size:
            return ref
        return ref.at[:, pl.ds(0, size)] if axis == 1 else ref.at[pl.ds(0, size)]

    loads = {
        "g1": load(first_gate, padded(g1, 1, units), 0),
        "u1": load(first_up, padded(u1, 1, units), 1),
        "d1": load(first_down, padded(d1, 0, units), 2),
        "wq": load(w_query, padded(wq, 1, inner), 3),
        "wk": load(w_key, padded(wk, 1, inner), 4),
        "wv": load(w_value, padded(wv, 1, inner), 5),
        "kc": load(keys, kc, 6),
        "vc": load(values, vc, 7),
        "wo": load(w_output, padded(wo, 0, inner), 8),
        "g2": load(last_gate, padded(g2, 1, units), 9),
        "u2": load(last_up, padded(u2, 1, units), 10),
        "d2": load(last_down, padded(d2, 0, units), 11),
    }

    def begin(*names):
        for name in names:
            loads[name].start()

    def finish(*names):
        for name in names:
            loads[name].wait()

    begin("g1", "u1")

    barrier = pltpu.get_barrier_semaphore()
    for i in range(1, n):
        pl.semaphore_signal(
            barrier, inc=1, device_id=(lax.rem(me_k + i, n), me_t), device_id_type=MESH
        )
    for i in range(1, t):
        pl.semaphore_signal(
            barrier, inc=1, device_id=(me_k, lax.rem(me_t + i, t)), device_id_type=MESH
        )

    for ref in (g1, u1, g2, u2):
        if ref.shape[1] > units:
            ref[:, units:] = jnp.zeros((ref.shape[0], ref.shape[1] - units), bf16)
    for ref in (d1, d2):
        if ref.shape[0] > units:
            ref[units:, :] = jnp.zeros((ref.shape[0] - units, ref.shape[1]), bf16)
    for ref in (wq, wk, wv):
        if ref.shape[1] > inner:
            ref[:, inner:] = jnp.zeros((ref.shape[0], ref.shape[1] - inner), bf16)
    if wo.shape[0] > inner:
        wo[inner:, :] = jnp.zeros((wo.shape[0] - inner, wo.shape[1]), bf16)

    flat = positions * heads
    row_head = lax.rem(lax.broadcasted_iota(jnp.int32, (2 * heads, flat), 0), heads)
    column = lax.broadcasted_iota(jnp.int32, (2 * heads, flat), 1)
    pos_ref[...] = jnp.where(
        lax.rem(column, heads) == row_head,
        column // heads + me_k * positions,
        jnp.int32(2**30),
    )

    pl.semaphore_wait(barrier, n + t - 2)

    def partner(me, size, step):
        if size & (size - 1):
            return lax.rem(me + step, size)
        other, bit = 0, 1
        while bit < size:
            digit = lax.rem(me // bit, 2)
            other = other + bit * (1 - digit if step & bit else digit)
            bit *= 2
        return other

    far_first = list(range(n - 1, -1, -1))
    kv_partner = [partner(me_k, n, i) if i else me_k for i in range(n)]
    tp_partner = [partner(me_t, t, i) if i else me_t for i in range(t)]
    if n & (n - 1):
        kv_source = [lax.rem(me_k + n - i, n) if i else me_k for i in range(n)]
    else:
        kv_source = kv_partner
    sends = []

    def ship(source, target, sem, index, axis):
        copy = pltpu.make_async_remote_copy(
            src_ref=source,
            dst_ref=target,
            send_sem=send_sem.at[len(sends)],
            recv_sem=sem,
            device_id=(index, me_t) if axis == "kv" else (me_k, index),
            device_id_type=MESH,
        )
        copy.start()
        sends.append(copy)

    def arrive(ref, sem):
        pltpu.make_async_remote_copy(
            src_ref=ref,
            dst_ref=ref,
            send_sem=send_sem.at[0],
            recv_sem=sem,
            device_id=(me_k, me_t),
            device_id_type=MESH,
        ).wait_recv()

    def broadcast(buffer, sems, axis):
        me, partners = (me_k, kv_partner) if axis == "kv" else (me_t, tp_partner)
        for peer in partners[:0:-1]:
            ship(buffer.at[me], buffer.at[me], sems.at[me], peer, axis)

    def await_all(buffer, sems, axis):
        me, size = (me_k, n) if axis == "kv" else (me_t, t)
        for i in range(1, size):
            source = lax.rem(me + size - i, size)
            arrive(buffer.at[source], sems.at[source])

    def dot(a, b):
        return jnp.dot(a, b, preferred_element_type=f32)

    lane = lax.broadcasted_iota(jnp.int32, (rows, LANE), 1)

    def norm_block(wide, gain):
        squares = jnp.sum(wide * wide, axis=1, keepdims=True)
        high = squares.astype(bf16)
        low = (squares - high.astype(f32)).astype(bf16)
        block = jnp.where(
            lane == 0, high.astype(f32), jnp.where(lane == 1, low.astype(f32), 0.0)
        ).astype(bf16)
        return block, (wide * gain[...]).astype(bf16)

    def inverse(block):
        return lax.rsqrt(jnp.sum(block, axis=1, keepdims=True) / cfg["model"] + epsilon)

    def scatter_products(wide, gain, weights, step, send, recv, sems):
        squares, scaled = norm_block(wide, gain)
        for i in far_first:
            owner = kv_partner[i]
            place = pl.ds(pl.multiple_of(owner * step, LANE), step)
            target = send.at[owner] if i else recv.at[me_k]
            for j, w in enumerate(weights):
                target[:, j * step : (j + 1) * step] = dot(scaled, w[:, place]).astype(bf16)
            target[:, len(weights) * step :] = squares
            if i:
                ship(send.at[owner], recv.at[me_k], sems.at[me_k], owner, "kv")

    def gather_sum(recv, sems):
        await_all(recv, sems, "kv")
        total = recv[0].astype(f32)
        for source in range(1, n):
            total += recv[source].astype(f32)
        return total

    def gated(wide, gain, gate, up, down, down_name, send, recv, sems, hid, hid_sems):
        scatter_products(wide, gain, (gate, up), span, send, recv, sems)
        total = gather_sum(recv, sems)
        inv = inverse(total[:, 2 * span :])
        a = total[:, :span] * inv
        b = total[:, span : 2 * span] * inv
        hid[me_k] = (a * (1.0 / (1.0 + jnp.exp(-a))) * b).astype(bf16)
        broadcast(hid, hid_sems, "kv")
        finish(down_name)
        return product_of_blocks(hid, hid_sems, down, span)

    def product_of_blocks(blocks, sems, weight, step):
        total = None
        for i in range(n):
            source = kv_source[i]
            if i:
                arrive(blocks.at[source], sems.at[source])
            place = pl.ds(pl.multiple_of(source * step, LANE), step)
            part = dot(blocks[source], weight[place, :])
            total = part if total is None else total + part
        return total

    def tp_total(part, buffer, sems):
        buffer[me_t] = part.astype(bf16)
        broadcast(buffer, sems, "tp")
        await_all(buffer, sems, "tp")
        total = buffer[0].astype(f32)
        for source in range(1, t):
            total += buffer[source].astype(f32)
        return total

    if gather_here:
        tok_all[me_t] = tokens[...]
        for i in range(1, t):
            ship(tokens, tok_all.at[me_t], tok_sem.at[me_t], lax.rem(me_t + i, t), "tp")
        await_all(tok_all, tok_sem, "tp")
        wide = jnp.concatenate([tok_all[s].astype(f32) for s in range(t)], axis=1)
    else:
        wide = tokens[...].astype(f32)

    finish("g1", "u1")
    begin("d1", "wq", "wk", "wv", "kc", "vc", "wo", "g2", "u2", "d2")

    part = gated(
        wide, first_gain, g1, u1, d1, "d1", gu_send1, gu_recv1, gu_sem1, hid1, hid_sem1
    )
    first = (wide + 0.5 * tp_total(part, down1, down_sem1)).astype(bf16).astype(f32)

    finish("wq", "wk", "wv")
    scatter_products(first, mixer_gain, (wq, wk, wv), head_span, qkv_send, qkv_recv, qkv_sem)
    total = gather_sum(qkv_recv, qkv_sem)
    inv = inverse(total[:, 3 * head_span :])
    query = (total[:, :head_span] * inv).astype(bf16)
    fresh_key = (total[:, head_span : 2 * head_span] * inv).astype(bf16).astype(f32)
    new_value = (total[:, 2 * head_span : 3 * head_span] * inv).astype(bf16).astype(f32)
    q_all[me_k] = query
    broadcast(q_all, q_sem, "kv")

    logit_scale = HEAD_DIM ** (-0.5)
    first_map = lane < HEAD_DIM
    await_all(q_all, q_sem, "kv")
    for h in range(heads):
        block = q_all[h // own_heads][:, (h % own_heads) * VAL_DIM : (h % own_heads + 1) * VAL_DIM]
        block = block.astype(f32) * logit_scale
        qf[:, h, :] = jnp.where(first_map, block, 0.0)
        qf[:, heads + h, :] = jnp.where(first_map, 0.0, block)

    finish("kc", "vc")
    wide_lane = lax.broadcasted_iota(jnp.int32, (2 * heads, LANE), 1)
    third = lax.rem(wide_lane, 3)
    map_row = lax.broadcasted_iota(jnp.int32, (2 * heads, LANE), 0) // heads
    slot = wide_lane - 6 * map_row

    def one_sequence(b, carry):
        score = lax.dot_general(
            qf[b].astype(bf16), kc[b], (((1,), (1,)), ((), ())), preferred_element_type=f32
        )
        score = jnp.where(pos_ref[...] < lengths[b], score, neg_fill)
        peak = jnp.max(score, axis=1, keepdims=True)
        weight = jnp.exp(score - peak)
        mass = jnp.sum(weight, axis=1, keepdims=True)
        acc[b, :, :LANE] = dot(weight.astype(bf16), vc[b])
        stats = jnp.where(slot < 0, 0.0, jnp.where(slot < 3, peak, jnp.where(slot < 6, mass, 0.0)))
        high = stats.astype(bf16).astype(f32)
        mid = (stats - high).astype(bf16).astype(f32)
        low = stats - high - mid
        acc[b, :, LANE:] = jnp.where(third == 0, high, jnp.where(third == 1, mid, low))
        return carry

    lax.fori_loop(0, rows, one_sequence, 0, unroll=2)

    pair_lane = lax.broadcasted_iota(jnp.int32, (rows, LANE), 1)
    for i in far_first:
        owner = kv_partner[i]
        target = att_send.at[owner] if i else att_recv.at[me_k]
        for c in range(own_heads):
            head = jnp.minimum(owner * own_heads + c, heads - 1)
            one, two = acc[:, head, :], acc[:, heads + head, :]
            place = pl.ds(c * rows, rows)
            target[place, :LANE] = one[:, :LANE].astype(bf16)
            target[place, LANE : 2 * LANE] = two[:, :LANE].astype(bf16)
            target[place, 2 * LANE :] = (one[:, LANE:] + two[:, LANE:]).astype(bf16)
        if i:
            ship(att_send.at[owner], att_recv.at[me_k], part_sem.at[me_k], owner, "kv")
    await_all(att_recv, part_sem, "kv")

    for c in range(own_heads):
        head = jnp.minimum(me_k * own_heads + c, heads - 1)
        lam_head = lam[head]
        cut = slice(c * VAL_DIM, (c + 1) * VAL_DIM)
        product = query[:, cut].astype(f32) * fresh_key[:, cut] * logit_scale
        maps = []
        for m in range(2):
            mine = first_map if m == 0 else jnp.logical_not(first_map)
            own = jnp.sum(jnp.where(mine, product, 0.0), axis=1, keepdims=True)
            place = pl.ds(c * rows, rows)
            peaks, masses = [], []
            highest = own
            for source in range(n):
                stats = att_recv[source, place, 2 * LANE :].astype(f32)
                is_peak = jnp.logical_and(pair_lane >= 6 * m, pair_lane < 6 * m + 3)
                is_mass = jnp.logical_and(pair_lane >= 6 * m + 3, pair_lane < 6 * m + 6)
                peaks.append(jnp.sum(jnp.where(is_peak, stats, 0.0), axis=1, keepdims=True))
                masses.append(jnp.sum(jnp.where(is_mass, stats, 0.0), axis=1, keepdims=True))
                highest = jnp.maximum(highest, peaks[-1])
            own_weight = jnp.exp(own - highest)
            den = own_weight
            num = own_weight.astype(bf16).astype(f32) * new_value[:, cut]
            for source in range(n):
                scale = jnp.exp(peaks[source] - highest)
                den += scale * masses[source]
                num += scale * att_recv[source, place, m * LANE : (m + 1) * LANE].astype(f32)
            maps.append(num / den)
        mixed = maps[0] - lam_head * maps[1]
        normed = (
            mixed
            * lax.rsqrt(jnp.mean(mixed * mixed, axis=1, keepdims=True) + epsilon)
            * head_gain[...]
        )
        att_all[me_k, :, cut] = normed.astype(bf16)
    broadcast(att_all, att_sem, "kv")
    finish("wo")
    part = product_of_blocks(att_all, att_sem, wo, head_span)
    second = (first + tp_total(part, out_all, out_sem)).astype(bf16).astype(f32)

    finish("g2", "u2")
    stream[...] = second
    part = gated(
        second, last_gain, g2, u2, d2, "d2", gu_send2, gu_recv2, gu_sem2, hid2, hid_sem2
    )
    if gather_here:
        for s in range(t):
            down2[s] = part[:, s * cols : (s + 1) * cols]
        for i in range(1, t):
            peer = lax.rem(me_t + i, t)
            ship(down2.at[peer], down2_recv.at[me_t], down_sem2.at[me_t], peer, "tp")
        down2_recv[me_t] = down2[me_t]
        await_all(down2_recv, down_sem2, "tp")
        total = down2_recv[0]
        for source in range(1, t):
            total += down2_recv[source]
        own = stream[:, pl.ds(pl.multiple_of(me_t * cols, LANE), cols)]
        result[...] = (own + 0.5 * total).astype(bf16)
    else:
        total = tp_total(part, down2, down_sem2)
        result[...] = (second + 0.5 * total).astype(bf16)
    for copy in sends:
        copy.wait_send()


def on_device(
    tokens,
    first_gain,
    first_gate,
    first_up,
    first_down,
    mixer_gain,
    w_query,
    w_key,
    w_value,
    w_output,
    lam_heads,
    head_gain,
    key_cache,
    value_cache,
    lengths,
    last_gain,
    last_gate,
    last_up,
    last_down,
):
    n, t = lax.axis_size("kv"), lax.axis_size("tp")
    rows, cols = tokens.shape
    width, units = first_gate.shape
    positions, heads = key_cache.shape[1:3]
    gather_here = cols % LANE == 0
    span = ceil_div(ceil_div(units, LANE), n) * LANE
    own_heads = ceil_div(heads, n)
    head_span = own_heads * VAL_DIM
    cfg = dict(
        n=n,
        t=t,
        width=width,
        model=width * n,
        rows=rows,
        cols=cols,
        units=units,
        heads=heads,
        positions=positions,
        span=span,
        own_heads=own_heads,
        gather_here=gather_here,
    )
    if not gather_here:
        tokens = lax.all_gather(tokens, "tp", axis=1, tiled=True)
    flat = positions * heads
    keys = key_cache.reshape(rows, flat, VAL_DIM)
    values = value_cache.reshape(rows, flat, VAL_DIM)

    gu = (n, rows, 2 * span + LANE)
    qkv = (n, rows, 3 * head_span + LANE)
    part_block = (n, own_heads * rows, 2 * VAL_DIM + LANE)
    down2_block = (t, rows, cols if gather_here else width)
    buffers = [
        ((width, n * span), bf16),
        ((width, n * span), bf16),
        ((n * span, width), bf16),
        ((width, n * head_span), bf16),
        ((width, n * head_span), bf16),
        ((width, n * head_span), bf16),
        ((n * head_span, width), bf16),
        ((rows, flat, VAL_DIM), bf16),
        ((rows, flat, VAL_DIM), bf16),
        ((width, n * span), bf16),
        ((width, n * span), bf16),
        ((n * span, width), bf16),
        ((t, rows, max(cols, LANE)), bf16),
        ((rows, width), f32),
        (gu, bf16),
        (gu, bf16),
        (gu, bf16),
        (gu, bf16),
        ((n, rows, span), bf16),
        ((n, rows, span), bf16),
        ((t, rows, width), bf16),
        (down2_block, f32 if gather_here else bf16),
        (down2_block, f32),
        (qkv, bf16),
        (qkv, bf16),
        ((n, rows, head_span), bf16),
        ((rows, 2 * heads, VAL_DIM), f32),
        ((rows, 2 * heads, VAL_DIM + LANE), f32),
        ((2 * heads, flat), jnp.int32),
        (part_block, bf16),
        (part_block, bf16),
        ((n, rows, head_span), bf16),
        ((t, rows, width), bf16),
    ]
    dma = pltpu.SemaphoreType.DMA
    sends = 8 * (n - 1) + 4 * (t - 1)
    sems = [12, sends, t, n, n, n, n, t, t, n, n, n, n, t]
    vmem = pl.BlockSpec(memory_space=pltpu.VMEM)
    smem = pl.BlockSpec(memory_space=pltpu.SMEM)
    hbm = pl.BlockSpec(memory_space=pl.ANY)
    return_cols = cols if gather_here else width
    result = pl.pallas_call(
        functools.partial(layer_kernel, cfg),
        out_shape=jax.ShapeDtypeStruct((rows, return_cols), bf16),
        in_specs=[vmem] * 5 + [smem] * 2 + [hbm] * 12,
        out_specs=vmem,
        scratch_shapes=[pltpu.VMEM(shape, kind) for shape, kind in buffers]
        + [dma((count,)) for count in sems],
        compiler_params=pltpu.CompilerParams(
            collective_id=0, has_side_effects=True, vmem_limit_bytes=60 * 2**20
        ),
    )(
        tokens,
        first_gain.reshape(1, width),
        mixer_gain.reshape(1, width),
        last_gain.reshape(1, width),
        head_gain.reshape(1, VAL_DIM),
        lam_heads,
        lengths,
        first_gate,
        first_up,
        first_down,
        w_query,
        w_key,
        w_value,
        w_output,
        keys,
        values,
        last_gate,
        last_up,
        last_down,
    )
    if not gather_here:
        result = lax.dynamic_slice_in_dim(result, lax.axis_index("tp") * cols, cols, 1)
    return result


def solution(mesh):
    return jax.shard_map(
        on_device,
        mesh=mesh,
        in_specs=(
            P(None, ("kv", "tp")),
            P("kv"),
            P("kv", "tp"),
            P("kv", "tp"),
            P("tp", "kv"),
            P("kv"),
            P("kv", "tp"),
            P("kv", "tp"),
            P("kv", "tp"),
            P("tp", "kv"),
            P("tp"),
            P(),
            P(None, "kv", "tp", None),
            P(None, "kv", "tp", None),
            P(),
            P("kv"),
            P("kv", "tp"),
            P("kv", "tp"),
            P("tp", "kv"),
        ),
        out_specs=P(None, ("kv", "tp")),
        check_vma=False,
    )
```

profile of v0, /device:TPU:0, one launch (start us, length us, event | category | flops | bytes accessed | tf_op | source)
XLA Modules:
  0.0 69.2 jit_solution(10677047278521216286)
XLA Ops:
  0.0 67.9 %shard_map.181 = bf16[16,128]{1,0:T(8,128)(2,1)} custom-call(bf16[16,128]{1,0:T(8,128)(2,1)} %tokens.1, f32[1,512]{1,0:T(1,128)} %bitcast.8, f32[1,512]{1,0:T(1,128)} %bitcast.9, f32[1,512]{1,0:T(1,128)} %bitcast.10, f32[1,128]{1,0:T(1,128)} %bitcast.11, f32[8]{0:T(128)} %lam.1, s32[16]{0:T(128)} %lengths.1, bf16[512,2816]{1,0:T(8,128)(2,1)} %first_gate.1, ...), custom_call_target="tpu_custom_call" | custom-call | tf_op jit(solution)/shard_map/pallas_call | solution.py:522
  67.9 1.3 %copy.21 = bf16[16,128]{1,0:T(8,128)(2,1)} copy(bf16[16,128]{1,0:T(8,128)(2,1)} %shard_map.181) | data formatting | bytes 8192
where the time goes:
time: 69.4 us; the launch traced here: 69.2 us
  Pallas kernels  67.9 us (98%)
  local copies, waits for them, and re-layouts  1.28 us (2%)
    pallas_call x1, Pallas kernels, on_device(): pl.pallas_call(functools.partial(layer_kernel, cfg), out_shape=jax.ShapeD...  67.9 us

commit v1 on v0

v1 whole, which is shorter than its diff:
```python
import functools

import jax
import jax.numpy as jnp
from jax import lax
from jax.experimental import pallas as pl
from jax.experimental.pallas import tpu as pltpu
from jax.sharding import PartitionSpec as P

HEAD_DIM = 64
VAL_DIM = 128
LANE = 128
epsilon = 1e-06
neg_fill = -1e30
bf16 = jnp.bfloat16
f32 = jnp.float32
MESH = pl.DeviceIdType.MESH


def ceil_div(a, b):
    return -(-a // b)


def layer_kernel(cfg, names, *refs):
    r = dict(zip(names, refs))
    n, t, rows = cfg["n"], cfg["t"], cfg["rows"]
    heads, positions = cfg["heads"], cfg["positions"]
    base, rem, lo, tiles = cfg["base"], cfg["rem"], cfg["lo"], cfg["tiles"]
    owners, per, first_owner = cfg["owners"], cfg["per"], cfg["first_owner"]
    cols, gather_here = cfg["cols"], cfg["gather_here"]
    chunks, chunk = cfg["chunks"], cfg["chunk"]
    units = cfg["units"]
    inner = heads * VAL_DIM
    share = per * VAL_DIM
    main = base * LANE
    me_k = lax.axis_index("kv")
    me_t = lax.axis_index("tp")
    halved = n & (n - 1) == 0

    load_count = [0]

    def load(source, target):
        load_count[0] += 1
        return pltpu.make_async_copy(source, target, r["load_sem"].at[load_count[0] - 1])

    def padded(ref, axis, size):
        if ref.shape[axis] == size:
            return ref
        return ref.at[:, pl.ds(0, size)] if axis == 1 else ref.at[pl.ds(0, size)]

    loads = {
        "tokens": load(r["tokens"], r["tok_all"].at[me_t] if gather_here else r["tok_in"]),
        "gain0": load(r["gain0_in"], r["gain0"]),
        "gain1": load(r["gain1_in"], r["gain1"]),
        "gain2": load(r["gain2_in"], r["gain2"]),
        "head_gain": load(r["head_gain_in"], r["head_gain"]),
        "lam": load(r["lam_in"], r["lam"]),
        "lengths": load(r["lengths_in"], r["lengths"]),
        "g1": load(r["first_gate"], padded(r["g1"], 1, units)),
        "u1": load(r["first_up"], padded(r["u1"], 1, units)),
        "d1": load(r["first_down"], padded(r["d1"], 0, units)),
        "wq": load(r["w_query"], r["wq"]),
        "wk": load(r["w_key"], r["wk"]),
        "wv": load(r["w_value"], r["wv"]),
        "kc": load(r["keys"], r["kc"]),
        "vc": load(r["values"], r["vc"]),
        "wo": load(r["w_output"], r["wo"]),
        "g2": load(r["last_gate"], padded(r["g2"], 1, units)),
        "u2": load(r["last_up"], padded(r["u2"], 1, units)),
        "d2": load(r["last_down"], padded(r["d2"], 0, units)),
    }

    def begin(*which):
        for name in which:
            loads[name].start()

    def finish(*which):
        for name in which:
            loads[name].wait()

    small = ("gain0", "gain1", "gain2", "head_gain", "lam", "lengths")
    begin("tokens", "g1", "u1", *small, "kc")

    barrier = pltpu.get_barrier_semaphore()
    for i in range(1, n):
        pl.semaphore_signal(
            barrier, inc=1, device_id=(lax.rem(me_k + i, n), me_t), device_id_type=MESH
        )
    for i in range(1, t):
        pl.semaphore_signal(
            barrier, inc=1, device_id=(me_k, lax.rem(me_t + i, t)), device_id_type=MESH
        )

    for name in ("g1", "u1", "g2", "u2"):
        ref = r[name]
        if ref.shape[1] > units:
            ref[:, units:] = jnp.zeros((ref.shape[0], ref.shape[1] - units), bf16)
    for name in ("d1", "d2"):
        ref = r[name]
        if ref.shape[0] > units:
            ref[units:, :] = jnp.zeros((ref.shape[0] - units, ref.shape[1]), bf16)

    flat = positions * heads
    row_head = lax.rem(lax.broadcasted_iota(jnp.int32, (2 * heads, flat), 0), heads)
    column = lax.broadcasted_iota(jnp.int32, (2 * heads, flat), 1)
    r["pos"][...] = jnp.where(
        lax.rem(column, heads) == row_head,
        column // heads + me_k * positions,
        jnp.int32(2**30),
    )
    pick_row = lax.broadcasted_iota(jnp.int32, (LANE, 4 * LANE), 0)
    pick_block = lax.broadcasted_iota(jnp.int32, (LANE, 4 * LANE), 1) // LANE
    r["pick"][...] = jnp.where(pick_row // 3 == pick_block, 1.0, 0.0).astype(bf16)

    finish("tokens")
    pl.semaphore_wait(barrier, n + t - 2)

    def partner(me, size, step):
        if size & (size - 1):
            return lax.rem(me + step, size)
        other, bit = 0, 1
        while bit < size:
            digit = lax.rem(me // bit, 2)
            other = other + bit * (1 - digit if step & bit else digit)
            bit *= 2
        return other

    far_first = list(range(n - 1, 0, -1))
    near_first = list(range(1, n))
    kv_partner = [partner(me_k, n, i) if i else me_k for i in range(n)]
    tp_partner = [partner(me_t, t, i) if i else me_t for i in range(t)]
    kv_source = kv_partner if halved else [lax.rem(me_k + n - i, n) for i in range(n)]
    sends = []

    def device(index, axis):
        return (index, me_t) if axis == "kv" else (me_k, index)

    def when(condition, action):
        if condition is None:
            action()
        else:
            pl.when(condition)(action)

    def ship(source, target, sem, index, axis, condition=None):
        copy = pltpu.make_async_remote_copy(
            src_ref=source,
            dst_ref=target,
            send_sem=r["send_sem"].at[len(sends)],
            recv_sem=sem,
            device_id=device(index, axis),
            device_id_type=MESH,
        )
        when(condition, copy.start)
        sends.append((copy, condition))

    def arrive(ref, sem):
        pltpu.make_async_remote_copy(
            src_ref=ref,
            dst_ref=ref,
            send_sem=r["send_sem"].at[0],
            recv_sem=sem,
            device_id=(me_k, me_t),
            device_id_type=MESH,
        ).wait_recv()

    def tp_broadcast(buffer, sems):
        for peer in tp_partner[:0:-1]:
            ship(buffer.at[me_t], buffer.at[me_t], sems.at[me_t], peer, "tp")

    def tp_await(buffer, sems):
        for i in range(1, t):
            source = lax.rem(me_t + t - i, t)
            arrive(buffer.at[source], sems.at[source])

    def dot(a, b):
        return jnp.dot(a, b, preferred_element_type=f32)

    def lanes(start, size):
        return pl.ds(pl.multiple_of(start, LANE), size)

    lane = lax.broadcasted_iota(jnp.int32, (rows, LANE), 1)
    diagonal = lane == lax.broadcasted_iota(jnp.int32, (rows, LANE), 0)

    def send_squares(wide, which):
        squares = jnp.sum(wide * wide, axis=1, keepdims=True)
        buffer, sems = r["squares"].at[which], r["sq_sem"].at[which]
        buffer[me_k] = jnp.sum(jnp.where(diagonal, squares, 0.0), axis=0, keepdims=True)
        for i in far_first:
            ship(buffer.at[me_k], buffer.at[me_k], sems.at[me_k], kv_partner[i], "kv")

    def inverse(which):
        buffer, sems = r["squares"].at[which], r["sq_sem"].at[which]
        for i in near_first:
            arrive(buffer.at[kv_source[i]], sems.at[kv_source[i]])
        total = buffer[0]
        for source in range(1, n):
            total += buffer[source]
        column_sum = jnp.sum(jnp.where(diagonal, total, 0.0), axis=1, keepdims=True)
        return lax.rsqrt(column_sum / cfg["model"] + epsilon)

    def scaled_by(wide, which):
        return (wide * r[f"gain{which}"][...]).astype(bf16)

    def start(owner):
        return owner * base + jnp.clip(owner - lo, 0, rem)

    def extra(owner):
        return jnp.logical_and(owner >= lo, owner < lo + rem)

    def gated(wide, which, gate, up, down, down_name, send, recv, sems, hid, hid_sems, fill):
        send_squares(wide, which)
        scaled = scaled_by(wide, which)
        order = far_first + [0]

        def part(owner, offset, size):
            place = lanes((start(owner) + offset) * LANE, size)
            return dot(scaled, gate[:, place]).astype(bf16), dot(scaled, up[:, place]).astype(bf16)

        if base:
            for i in order:
                owner = kv_partner[i]
                target = send.at[owner] if i else recv.at[me_k]
                g, u = part(owner, 0, main)
                target[:, :main] = g
                target[:, main : 2 * main] = u
                if i:
                    cut = pl.ds(0, 2 * main)
                    ship(
                        send.at[owner, :, cut],
                        recv.at[me_k, :, cut],
                        sems.at[0, me_k],
                        owner,
                        "kv",
                    )
        if rem:
            for i in order:
                owner = kv_partner[i]
                target = send.at[owner] if i else recv.at[me_k]
                g, u = part(owner, base, LANE)
                target[:, 2 * main : 2 * main + LANE] = g
                target[:, 2 * main + LANE :] = u
                if i:
                    cut = pl.ds(2 * main, 2 * LANE)
                    ship(
                        send.at[owner, :, cut],
                        recv.at[me_k, :, cut],
                        sems.at[1, me_k],
                        owner,
                        "kv",
                        extra(owner),
                    )
        fill()
        inv = inverse(which)

        def activate(index, begin_at, size):
            cut = slice(begin_at, begin_at + 2 * size)
            total = recv[me_k, :, cut].astype(f32)
            for i in near_first:
                source = kv_source[i]
                arrive(recv.at[source, :, pl.ds(begin_at, 2 * size)], sems.at[index, source])
                total += recv[source, :, cut].astype(f32)
            a = total[:, :size] * inv
            b = total[:, size:] * inv
            return (a * (1.0 / (1.0 + jnp.exp(-a))) * b).astype(bf16)

        my_main = lanes(start(me_k) * LANE, main) if base else None
        my_extra = lanes((start(me_k) + base) * LANE, LANE)
        mine = extra(me_k)
        if base:
            hid[:, my_main] = activate(0, 0, main)
            for i in far_first:
                ship(
                    hid.at[:, my_main],
                    hid.at[:, my_main],
                    hid_sems.at[0, me_k],
                    kv_partner[i],
                    "kv",
                )
        if rem:

            def do_extra():
                hid[:, my_extra] = activate(1, 2 * main, LANE)

            pl.when(mine)(do_extra)
            for i in far_first:
                ship(
                    hid.at[:, my_extra],
                    hid.at[:, my_extra],
                    hid_sems.at[1, me_k],
                    kv_partner[i],
                    "kv",
                    mine,
                )
        finish(down_name)

        def hid_arrive(indices):
            for i in indices:
                source = kv_source[i]
                if base:
                    place = lanes(start(source) * LANE, main)
                    arrive(hid.at[:, place], hid_sems.at[0, source])
            for i in indices:
                source = kv_source[i]
                if rem:
                    place = lanes((start(source) + base) * LANE, LANE)

                    def wait_extra():
                        arrive(hid.at[:, place], hid_sems.at[1, source])

                    pl.when(extra(source))(wait_extra)

        half_tiles = (n // 2) * base + min(max(n // 2 - lo, 0), rem)
        if halved and n > 1 and half_tiles * 2 == tiles:
            size = half_tiles * LANE
            near = jnp.where(me_k < n // 2, 0, size)
            hid_arrive(range(1, n // 2))
            total = dot(hid[:, lanes(near, size)], down[lanes(near, size), :])
            hid_arrive(range(n // 2, n))
            far = size - near
            return total + dot(hid[:, lanes(far, size)], down[lanes(far, size), :])
        hid_arrive(near_first)
        size = tiles * LANE
        return dot(hid[:, :size], down[...])

    def tp_total(part, buffer, sems):
        buffer[me_t] = part.astype(bf16)
        tp_broadcast(buffer, sems)
        tp_await(buffer, sems)
        total = buffer[0].astype(f32)
        for source in range(1, t):
            total += buffer[source].astype(f32)
        return total

    if gather_here:
        tok_all = r["tok_all"]
        for i in range(t - 1, 0, -1):
            ship(tok_all.at[me_t], tok_all.at[me_t], r["tok_sem"].at[me_t], tp_partner[i], "tp")
    begin("d1", "wq", "wk", "wv", "vc", "wo", "g2", "u2", "d2")
    finish("g1", "u1", *small)
    if gather_here:
        tp_await(tok_all, r["tok_sem"])
        wide = jnp.concatenate([tok_all[s].astype(f32) for s in range(t)], axis=1)
    else:
        wide = r["tok_in"][...].astype(f32)

    def nothing():
        pass

    def turn_keys(lower, upper):
        kc, kt = r["kc"], r["kt"]

        def one(b, carry):
            kt[b] = kc[b].T
            return carry

        lax.fori_loop(lower, upper, one, 0, unroll=2)

    def first_fill():
        if cfg["turned"]:
            finish("kc")
            turn_keys(0, rows)

    part = gated(
        wide,
        0,
        r["g1"],
        r["u1"],
        r["d1"],
        "d1",
        r["gu_send1"],
        r["gu_recv1"],
        r["gu_sem1"],
        r["hid1"],
        r["hid_sem1"],
        first_fill,
    )
    first = (wide + 0.5 * tp_total(part, r["down1"], r["down_sem1"])).astype(bf16).astype(f32)

    finish("wq")
    send_squares(first, 1)
    scaled = scaled_by(first, 1)
    query_part = dot(scaled, r["wq"][...]).astype(bf16)
    q_send, q_recv, q_sem = r["q_send"], r["q_recv"], r["q_sem"]
    for c in range(chunks):
        q_send[c] = query_part[c * chunk : (c + 1) * chunk]
    for c in range(chunks):
        for i in far_first:
            ship(q_send.at[c], q_recv.at[me_k, c], q_sem.at[me_k, c], kv_partner[i], "kv")

    kv_send, kv_recv, kv_sem = r["kv_send"], r["kv_recv"], r["kv_sem"]
    finish("wk", "wv")
    key_part = dot(scaled, r["wk"][...]).astype(bf16)
    value_part = dot(scaled, r["wv"][...]).astype(bf16)
    shift = jnp.where(me_k < n // 2, owners // 2, 0)
    my_place = me_k - first_owner
    is_owner = jnp.logical_and(my_place >= 0, my_place < owners)
    my_slot = jnp.clip(my_place, 0, owners - 1)
    for j in range(owners):
        kv_send[j, :, :share] = key_part[:, j * share : (j + 1) * share]
        kv_send[j, :, share:] = value_part[:, j * share : (j + 1) * share]
    owner_order = [lax.rem(j + shift, owners) for j in range(owners)]
    for j in owner_order:
        owner = j + first_owner
        ship(kv_send.at[j], kv_recv.at[me_k], kv_sem.at[me_k], owner, "kv", me_k != owner)

    inv = inverse(1)
    logit_scale = HEAD_DIM ** (-0.5)
    wide_lane = lax.broadcasted_iota(jnp.int32, (2 * heads, LANE), 1)
    third = lax.rem(wide_lane, 3)
    map_row = lax.broadcasted_iota(jnp.int32, (2 * heads, LANE), 0) // heads
    slot = wide_lane - 6 * map_row
    first_half = lax.broadcasted_iota(jnp.int32, (chunk, LANE), 1) < HEAD_DIM
    finish("vc")
    if not cfg["turned"]:
        finish("kc")
    kc, vc, kt, qf, acc, q_all = r["kc"], r["vc"], r["kt"], r["qf"], r["acc"], r["q_all"]
    score_ref, pos, lengths = r["score"], r["pos"], r["lengths"]
    att_send, att_recv, part_sem = r["att_send"], r["att_recv"], r["part_sem"]

    def attend(c):
        total = q_send[c].astype(f32)
        for i in near_first:
            source = kv_source[i]
            arrive(q_recv.at[source, c], q_sem.at[source, c])
            total += q_recv[source, c].astype(f32)
        query = (total * inv[c * chunk : (c + 1) * chunk]).astype(bf16)
        q_all[c * chunk : (c + 1) * chunk, :] = query.astype(f32)
        for h in range(heads):
            block = query[:, h * VAL_DIM : (h + 1) * VAL_DIM].astype(f32) * logit_scale
            qf[:, h, :] = jnp.where(first_half, block, 0.0)
            qf[:, heads + h, :] = jnp.where(first_half, 0.0, block)
        for i in range(chunk):
            b = c * chunk + i
            if cfg["turned"]:
                score_ref[i] = dot(qf[i].astype(bf16), kt[b])
            else:
                score_ref[i] = lax.dot_general(
                    qf[i].astype(bf16),
                    kc[b],
                    (((1,), (1,)), ((), ())),
                    preferred_element_type=f32,
                )
        for i in range(chunk):
            b = c * chunk + i
            score = jnp.where(pos[...] < lengths[b], score_ref[i], neg_fill)
            peak = jnp.max(score, axis=1, keepdims=True)
            weight = jnp.exp(score - peak)
            mass = jnp.sum(weight, axis=1, keepdims=True)
            acc[i, :, :LANE] = dot(weight.astype(bf16), vc[b])
            stats = jnp.where(
                slot < 0, 0.0, jnp.where(slot < 3, peak, jnp.where(slot < 6, mass, 0.0))
            )
            high = stats.astype(bf16).astype(f32)
            mid = (stats - high).astype(bf16).astype(f32)
            low = stats - high - mid
            acc[i, :, LANE:] = jnp.where(third == 0, high, jnp.where(third == 1, mid, low))
        for j in range(owners):
            for p in range(per):
                head = j * per + p
                one, two = acc[:, head, :], acc[:, heads + head, :]
                place = pl.ds(p * chunk, chunk)
                att_send[c, j, place, :LANE] = one[:, :LANE].astype(bf16)
                att_send[c, j, place, LANE : 2 * LANE] = two[:, :LANE].astype(bf16)
                att_send[c, j, place, 2 * LANE :] = (one[:, LANE:] + two[:, LANE:]).astype(bf16)
        for j in owner_order:
            owner = j + first_owner
            ship(
                att_send.at[c, j],
                att_recv.at[me_k, c],
                part_sem.at[me_k, c],
                owner,
                "kv",
                me_k != owner,
            )

    for c in range(chunks):
        attend(c)

    att_all, att_sem = r["att_all"], r["att_sem"]
    my_share = lanes(my_slot * share, share)
    half = lax.broadcasted_iota(jnp.int32, (per * chunk, LANE), 1) < HEAD_DIM

    def combine():
        kv_recv[me_k] = kv_send[my_slot]
        for i in near_first:
            source = kv_source[i]
            arrive(kv_recv.at[source], kv_sem.at[source])
        fresh = kv_recv[0].astype(f32)
        for source in range(1, n):
            fresh += kv_recv[source].astype(f32)
        fresh = (fresh * inv).astype(bf16).astype(f32)
        fresh_key, fresh_value = fresh[:, :share], fresh[:, share:]
        query = q_all[:, my_share]
        product = query * fresh_key * logit_scale

        def stacked(x, c):
            return jnp.concatenate(
                [
                    x[c * chunk : (c + 1) * chunk, p * VAL_DIM : (p + 1) * VAL_DIM]
                    for p in range(per)
                ],
                axis=0,
            )

        own = []
        for c in range(chunks):
            block = stacked(product, c)
            own.append(
                [
                    jnp.sum(jnp.where(half, block, 0.0), axis=1, keepdims=True),
                    jnp.sum(jnp.where(half, 0.0, block), axis=1, keepdims=True),
                ]
            )
        lam_rows = jnp.concatenate(
            [jnp.full((chunk, LANE), r["lam"][my_slot * per + p], f32) for p in range(per)], axis=0
        )
        for c in range(chunks):
            att_recv[me_k, c] = att_send[c, my_slot]
            for i in near_first:
                source = kv_source[i]
                arrive(att_recv.at[source, c], part_sem.at[source, c])
            stats = jnp.concatenate(
                [att_recv[source, c, :, 2 * LANE :] for source in range(n)], axis=0
            )
            stats = dot(stats, r["pick"][...])
            high = per * chunk
            new_value = stacked(fresh_value, c)
            maps = []
            for m in range(2):
                peaks = [
                    stats[s * high : (s + 1) * high, 2 * m * LANE : (2 * m + 1) * LANE]
                    for s in range(n)
                ]
                masses = [
                    stats[s * high : (s + 1) * high, (2 * m + 1) * LANE : (2 * m + 2) * LANE]
                    for s in range(n)
                ]
                highest = jnp.broadcast_to(own[c][m], (high, LANE))
                for peak in peaks:
                    highest = jnp.maximum(highest, peak)
                own_weight = jnp.exp(own[c][m] - highest)
                den = own_weight
                num = own_weight.astype(bf16).astype(f32) * new_value
                for source in range(n):
                    scale = jnp.exp(peaks[source] - highest)
                    den += scale * masses[source]
                    num += scale * att_recv[source, c, :, m * LANE : (m + 1) * LANE].astype(f32)
                maps.append(num / den)
            mixed = maps[0] - lam_rows * maps[1]
            normed = (
                mixed
                * lax.rsqrt(jnp.mean(mixed * mixed, axis=1, keepdims=True) + epsilon)
                * r["head_gain"][...]
            )
            for p in range(per):
                r["att_own"][c * chunk : (c + 1) * chunk, p * VAL_DIM : (p + 1) * VAL_DIM] = (
                    normed[p * chunk : (p + 1) * chunk]
                )
        att_all[:, my_share] = r["att_own"][...].astype(bf16)

    pl.when(is_owner)(combine)
    for i in far_first:
        ship(
            att_all.at[:, my_share],
            att_all.at[:, my_share],
            att_sem.at[my_slot],
            kv_partner[i],
            "kv",
            is_owner,
        )
    finish("wo")

    def att_arrive(j):
        place = lanes(j * share, share)

        def wait_share():
            arrive(att_all.at[:, place], att_sem.at[j])

        pl.when(me_k != j + first_owner)(wait_share)

    wo = r["wo"]
    if halved and owners % 2 == 0 and 2 * first_owner + owners == n:
        size = owners // 2 * share
        near_low = me_k < n // 2
        near_slot = jnp.where(near_low, 0, owners // 2)
        far_slot = owners // 2 - near_slot
        for j in range(owners // 2):
            att_arrive(near_slot + j)
        near = near_slot * share
        part = dot(att_all[:, lanes(near, size)], wo[lanes(near, size), :])
        for j in range(owners // 2):
            att_arrive(far_slot + j)
        far = far_slot * share
        part += dot(att_all[:, lanes(far, size)], wo[lanes(far, size), :])
    else:
        for j in range(owners):
            att_arrive(jnp.int32(j))
        part = dot(att_all[...], wo[...])
    second = (first + tp_total(part, r["out_all"], r["out_sem"])).astype(bf16).astype(f32)

    finish("g2", "u2")
    stream, result = r["stream"], r["result"]
    stream[...] = second
    part = gated(
        second,
        2,
        r["g2"],
        r["u2"],
        r["d2"],
        "d2",
        r["gu_send2"],
        r["gu_recv2"],
        r["gu_sem2"],
        r["hid2"],
        r["hid_sem2"],
        nothing,
    )
    if gather_here:
        down2, down2_recv, sems = r["down2"], r["down2_recv"], r["down_sem2"]
        for s in range(t):
            down2[s] = part[:, s * cols : (s + 1) * cols]
        for peer in tp_partner[:0:-1]:
            ship(down2.at[peer], down2_recv.at[me_t], sems.at[me_t], peer, "tp")
        down2_recv[me_t] = down2[me_t]
        tp_await(down2_recv, sems)
        total = down2_recv[0]
        for source in range(1, t):
            total += down2_recv[source]
        own = stream[:, lanes(me_t * cols, cols)]
        result[...] = (own + 0.5 * total).astype(bf16)
    else:
        total = tp_total(part, r["down2"], r["down_sem2"])
        result[...] = (second + 0.5 * total).astype(bf16)
    for copy, condition in sends:
        when(condition, copy.wait_send)


def on_device(
    tokens,
    first_gain,
    first_gate,
    first_up,
    first_down,
    mixer_gain,
    w_query,
    w_key,
    w_value,
    w_output,
    lam_heads,
    head_gain,
    key_cache,
    value_cache,
    lengths,
    last_gain,
    last_gate,
    last_up,
    last_down,
):
    n, t = lax.axis_size("kv"), lax.axis_size("tp")
    rows, cols = tokens.shape
    width, units = first_gate.shape
    positions, heads = key_cache.shape[1:3]
    gather_here = cols % LANE == 0
    tiles = ceil_div(units, LANE)
    base, rem = divmod(tiles, n)
    lo = (n - rem) // 2
    owners = heads // 2 if heads % 2 == 0 and heads // 2 <= n else heads
    per = heads // owners
    chunks = 2 if rows % 16 == 0 else 1
    chunk = rows // chunks
    inner = heads * VAL_DIM
    share = per * VAL_DIM
    cfg = dict(
        n=n,
        t=t,
        model=width * n,
        rows=rows,
        cols=cols,
        units=units,
        heads=heads,
        positions=positions,
        tiles=tiles,
        base=base,
        rem=rem,
        lo=lo,
        owners=owners,
        per=per,
        first_owner=(n - owners) // 2,
        gather_here=gather_here,
        chunks=chunks,
        chunk=chunk,
        turned=TURNED,
    )
    if not gather_here:
        tokens = lax.all_gather(tokens, "tp", axis=1, tiled=True)
    flat = positions * heads
    keys = key_cache.reshape(rows, flat, VAL_DIM)
    values = value_cache.reshape(rows, flat, VAL_DIM)

    wide_units = (tiles + (1 if rem else 0)) * LANE
    gu = (n, rows, 2 * (base + (1 if rem else 0)) * LANE)
    dma = pltpu.SemaphoreType.DMA
    return_cols = cols if gather_here else width
    inputs = dict(
        tokens=tokens,
        gain0_in=first_gain.reshape(1, width),
        gain1_in=mixer_gain.reshape(1, width),
        gain2_in=last_gain.reshape(1, width),
        head_gain_in=head_gain.reshape(1, VAL_DIM),
        lam_in=lam_heads,
        lengths_in=lengths,
        first_gate=first_gate,
        first_up=first_up,
        first_down=first_down,
        w_query=w_query,
        w_key=w_key,
        w_value=w_value,
        w_output=w_output,
        keys=keys,
        values=values,
        last_gate=last_gate,
        last_up=last_up,
        last_down=last_down,
    )
    scratch = dict(
        gain0=((1, width), f32),
        gain1=((1, width), f32),
        gain2=((1, width), f32),
        head_gain=((1, VAL_DIM), f32),
        g1=((width, wide_units), bf16),
        u1=((width, wide_units), bf16),
        d1=((tiles * LANE, width), bf16),
        wq=((width, inner), bf16),
        wk=((width, inner), bf16),
        wv=((width, inner), bf16),
        wo=((inner, width), bf16),
        kc=((rows, flat, VAL_DIM), bf16),
        vc=((rows, flat, VAL_DIM), bf16),
        kt=((rows, VAL_DIM, flat) if TURNED else (1, VAL_DIM, LANE), bf16),
        g2=((width, wide_units), bf16),
        u2=((width, wide_units), bf16),
        d2=((tiles * LANE, width), bf16),
        stream=((rows, width), f32),
        squares=((3, n, 1, LANE), f32),
        gu_send1=(gu, bf16),
        gu_recv1=(gu, bf16),
        gu_send2=(gu, bf16),
        gu_recv2=(gu, bf16),
        hid1=((rows, wide_units), bf16),
        hid2=((rows, wide_units), bf16),
        down1=((t, rows, width), bf16),
        out_all=((t, rows, width), bf16),
        q_send=((chunks, chunk, inner), bf16),
        q_recv=((n, chunks, chunk, inner), bf16),
        q_all=((rows, inner), f32),
        kv_send=((owners, rows, 2 * share), bf16),
        kv_recv=((n, rows, 2 * share), bf16),
        qf=((chunk, 2 * heads, VAL_DIM), f32),
        score=((chunk, 2 * heads, flat), f32),
        acc=((chunk, 2 * heads, VAL_DIM + LANE), f32),
        pos=((2 * heads, flat), jnp.int32),
        pick=((LANE, 4 * LANE), bf16),
        att_send=((chunks, owners, per * chunk, 2 * VAL_DIM + LANE), bf16),
        att_recv=((n, chunks, per * chunk, 2 * VAL_DIM + LANE), bf16),
        att_own=((rows, share), f32),
        att_all=((rows, inner), bf16),
    )
    if gather_here:
        scratch.update(
            tok_all=((t, rows, cols), bf16),
            down2=((t, rows, cols), f32),
            down2_recv=((t, rows, cols), f32),
        )
    else:
        scratch.update(tok_in=((rows, width), bf16), down2=((t, rows, width), bf16))
    sends = (n - 1) * (3 + 8 + chunks + 1) + owners * (1 + chunks) + 4 * (t - 1)
    sems = dict(
        load_sem=(19,),
        send_sem=(sends,),
        tok_sem=(t,),
        sq_sem=(3, n),
        gu_sem1=(2, n),
        gu_sem2=(2, n),
        hid_sem1=(2, n),
        hid_sem2=(2, n),
        down_sem1=(t,),
        down_sem2=(t,),
        out_sem=(t,),
        q_sem=(n, chunks),
        kv_sem=(n,),
        part_sem=(n, chunks),
        att_sem=(owners,),
    )
    smem = dict(lam=(lam_heads.shape, f32), lengths=(lengths.shape, jnp.int32))
    names = [*inputs, "result", *scratch, *smem, *sems]
    result = pl.pallas_call(
        functools.partial(layer_kernel, cfg, names),
        out_shape=pltpu.VMEM((rows, return_cols), bf16),
        in_specs=[pl.BlockSpec(memory_space=pl.ANY)] * len(inputs),
        out_specs=pl.BlockSpec(memory_space=pltpu.VMEM),
        scratch_shapes=[pltpu.VMEM(shape, kind) for shape, kind in scratch.values()]
        + [pltpu.SMEM(shape, kind) for shape, kind in smem.values()]
        + [dma(shape) for shape in sems.values()],
        compiler_params=pltpu.CompilerParams(
            collective_id=0, has_side_effects=True, vmem_limit_bytes=63 * 2**20
        ),
    )(*inputs.values())
    if not gather_here:
        result = lax.dynamic_slice_in_dim(result, lax.axis_index("tp") * cols, cols, 1)
    return result


TURNED = True


def solution(mesh):
    return jax.shard_map(
        on_device,
        mesh=mesh,
        in_specs=(
            P(None, ("kv", "tp")),
            P("kv"),
            P("kv", "tp"),
            P("kv", "tp"),
            P("tp", "kv"),
            P("kv"),
            P("kv", "tp"),
            P("kv", "tp"),
            P("kv", "tp"),
            P("tp", "kv"),
            P("tp"),
            P(),
            P(None, "kv", "tp", None),
            P(None, "kv", "tp", None),
            P(),
            P("kv"),
            P("kv", "tp"),
            P("kv", "tp"),
            P("tp", "kv"),
        ),
        out_specs=P(None, ("kv", "tp")),
        check_vma=False,
    )
```

time: 69.4 us -> 60.3 us (0.87)
  Pallas kernels: 67.9 us -> 59.5 us
    pallas_call x1, Pallas kernels: 67.9 us -> 59.5 us  [on_device(): pl.pallas_call(functools.partial(layer_kernel, cfg, names), out_shape=plt...]
where the time goes in v1:
time: 60.3 us; the launch traced here: 60.1 us
  Pallas kernels  59.5 us (99%)
    pallas_call x1, Pallas kernels, on_device(): pl.pallas_call(functools.partial(layer_kernel, cfg, names), out_shape=plt...  59.5 us

profile of v1, /device:TPU:0, one launch (start us, length us, event | category | flops | bytes accessed | tf_op | source)
XLA Modules:
  0.0 60.1 jit_solution(9321715138525167528)
XLA Ops:
  0.0 59.5 %shard_map.181 = bf16[16,128]{1,0:T(8,128)(2,1)S(1)} custom-call(bf16[16,128]{1,0:T(8,128)(2,1)} %refs_0_.1, f32[1,512]{1,0:T(1,128)} %bitcast.8, f32[1,512]{1,0:T(1,128)} %bitcast.9, f32[1,512]{1,0:T(1,128)} %bitcast.10, f32[1,128]{1,0:T(1,128)} %bitcast.11, f32[8]{0:T(128)} %refs_5_.1, s32[16]{0:T(128)} %refs_6_.1, bf16[512,2816]{1,0:T(8,128)(2,1)} %refs_7_.1, ...), custom_call_target="tpu_custom_call" | custom-call | tf_op jit(solution)/shard_map/pallas_call | solution.py:796
  59.5 0.6 copy.21

commit v2 on v1

v2 whole, which is shorter than its diff:
```python
import functools
import types

import jax
import jax.numpy as jnp
from jax import lax
from jax.experimental import pallas as pl
from jax.experimental.pallas import tpu as pltpu
from jax.sharding import PartitionSpec as P

HEAD_DIM = 64
VAL_DIM = 128
LANE = 128
epsilon = 1e-06
neg_fill = -1e30
bf16 = jnp.bfloat16
f32 = jnp.float32
MESH = pl.DeviceIdType.MESH


def ceil_div(a, b):
    return -(-a // b)


def layer_kernel(cfg, names, *refs):
    r = types.SimpleNamespace(**dict(zip(names, refs)))
    n, t, rows = cfg.n, cfg.t, cfg.rows
    heads, positions = cfg.heads, cfg.positions
    base, rem, lo, tiles = cfg.base, cfg.rem, cfg.lo, cfg.tiles
    owners, per, first_owner = cfg.owners, cfg.per, cfg.first_owner
    cols, gather_here = cfg.cols, cfg.gather_here
    chunks, chunk = cfg.chunks, cfg.chunk
    units = cfg.units
    inner = heads * VAL_DIM
    share = per * VAL_DIM
    main = base * LANE
    me_k = lax.axis_index("kv")
    me_t = lax.axis_index("tp")
    halved = n & (n - 1) == 0

    load_count = [0]

    def load(source, target):
        load_count[0] += 1
        return pltpu.make_async_copy(source, target, r.load_sem.at[load_count[0] - 1])

    def padded(ref, axis, size):
        if ref.shape[axis] == size:
            return ref
        return ref.at[:, pl.ds(0, size)] if axis == 1 else ref.at[pl.ds(0, size)]

    loads = types.SimpleNamespace(
        tokens=load(r.tokens, r.tok_all.at[me_t] if gather_here else r.tok_in),
        gain0=load(r.gain0_in, r.gain0),
        gain1=load(r.gain1_in, r.gain1),
        gain2=load(r.gain2_in, r.gain2),
        head_gain=load(r.head_gain_in, r.head_gain),
        lam=load(r.lam_in, r.lam),
        lengths=load(r.lengths_in, r.lengths),
        g1=load(r.first_gate, padded(r.g1, 1, units)),
        u1=load(r.first_up, padded(r.u1, 1, units)),
        d1=load(r.first_down, padded(r.d1, 0, units)),
        wq=load(r.w_query, r.wq),
        wk=load(r.w_key, r.wk),
        wv=load(r.w_value, r.wv),
        kc=load(r.keys, r.kc),
        vc=load(r.values, r.vc),
        wo=load(r.w_output, r.wo),
        g2=load(r.last_gate, padded(r.g2, 1, units)),
        u2=load(r.last_up, padded(r.u2, 1, units)),
        d2=load(r.last_down, padded(r.d2, 0, units)),
    )

    def begin(*which):
        for copy in which:
            copy.start()

    def finish(*which):
        for copy in which:
            copy.wait()

    small = (loads.gain0, loads.gain1, loads.gain2, loads.head_gain, loads.lam, loads.lengths)
    begin(loads.tokens, loads.g1, loads.u1, *small, loads.kc)

    def when(condition, action):
        if condition is None:
            action()
        else:
            pl.when(condition)(action)

    staged = n % 2 == 0 and 2 < n <= 8
    level, side, levels = me_k // 2, lax.rem(me_k, 2), n // 2
    barrier = pltpu.get_barrier_semaphore()

    def greet(sem, ranks):
        for rank, condition in ranks:

            def signal():
                pl.semaphore_signal(sem, inc=1, device_id=(rank, me_t), device_id_type=MESH)

            when(condition, signal)

    def count(ranks):
        total = jnp.int32(0)
        for _, condition in ranks:
            total += 1 if condition is None else condition.astype(jnp.int32)
        return total

    def reach(step, flip):
        if step == 0:
            return [(level * 2 + 1 - side, None)]
        to_side = 1 - side if flip else side
        return [
            ((level - step) * 2 + to_side, level >= step),
            ((level + step) * 2 + to_side, level < levels - step),
        ]

    if staged:
        adjacent = reach(0, True) + reach(1, False)
        within = adjacent + reach(1, True) + (reach(2, False) if levels > 2 else [])
    else:
        adjacent = [(lax.rem(me_k + i, n), None) for i in range(1, n)]
    greet(barrier, adjacent)
    for i in range(1, t):
        pl.semaphore_signal(
            barrier, inc=1, device_id=(me_k, lax.rem(me_t + i, t)), device_id_type=MESH
        )

    finish(loads.tokens)
    pl.semaphore_wait(barrier, count(adjacent) + (t - 1))

    def partner(me, size, step):
        if size & (size - 1):
            return lax.rem(me + step, size)
        other, bit = 0, 1
        while bit < size:
            digit = lax.rem(me // bit, 2)
            other = other + bit * (1 - digit if step & bit else digit)
            bit *= 2
        return other

    far_first = list(range(n - 1, 0, -1))
    near_first = list(range(1, n))
    kv_partner = [partner(me_k, n, i) if i else me_k for i in range(n)]
    tp_partner = [partner(me_t, t, i) if i else me_t for i in range(t)]
    kv_source = kv_partner if halved else [lax.rem(me_k + n - i, n) for i in range(n)]
    sends = []
    groups = []

    def device(index, axis):
        return (index, me_t) if axis == "kv" else (me_k, index)

    def ship(copies, sem, axis, keep=None):
        own = r.send_sem.at[len(groups)]
        if keep is None:
            groups.append(len(copies))
        for source, target, index, condition in copies:
            copy = pltpu.make_async_remote_copy(
                src_ref=source,
                dst_ref=target,
                send_sem=own,
                recv_sem=sem,
                device_id=device(index, axis),
                device_id_type=MESH,
            )
            when(condition, copy.start)
        return own

    def sent(own, ref, condition=None):
        copy = pltpu.make_async_remote_copy(
            src_ref=ref,
            dst_ref=ref,
            send_sem=own,
            recv_sem=own,
            device_id=(me_k, me_t),
            device_id_type=MESH,
        )
        sends.append((copy, condition))

    def arrive(ref, sem):
        pltpu.make_async_remote_copy(
            src_ref=ref,
            dst_ref=ref,
            send_sem=sem,
            recv_sem=sem,
            device_id=(me_k, me_t),
            device_id_type=MESH,
        ).wait_recv()

    def kv_broadcast(ref, sem):
        return ship([(ref, ref, kv_partner[i], None) for i in far_first], sem, "kv")

    def tp_broadcast(buffer, sem):
        block = buffer.at[me_t]
        own = ship([(block, block, peer, None) for peer in tp_partner[:0:-1]], sem, "tp")
        sent(own, buffer.at[pl.ds(0, t - 1)])

    def tp_await(buffer, sem):
        arrive(buffer.at[pl.ds(0, t - 1)], sem)

    def dot(a, b):
        return jnp.dot(a, b, preferred_element_type=f32)

    def lanes(start, size):
        return pl.ds(pl.multiple_of(start, LANE), size)

    lane = lax.broadcasted_iota(jnp.int32, (rows, LANE), 1)
    diagonal = lane == lax.broadcasted_iota(jnp.int32, (rows, LANE), 0)

    def send_squares(wide, which):
        squares = jnp.sum(wide * wide, axis=1, keepdims=True)
        buffer, sems = r.squares.at[which], r.sq_sem.at[which]
        buffer[me_k] = jnp.sum(jnp.where(diagonal, squares, 0.0), axis=0, keepdims=True)
        own = kv_broadcast(buffer.at[me_k], sems)
        sent(own, buffer.at[pl.ds(0, n - 1)])

    def inverse(which):
        buffer, sems = r.squares.at[which], r.sq_sem.at[which]
        arrive(buffer.at[pl.ds(0, n - 1)], sems)
        total = buffer[0]
        for source in range(1, n):
            total += buffer[source]
        column_sum = jnp.sum(jnp.where(diagonal, total, 0.0), axis=1, keepdims=True)
        return lax.rsqrt(column_sum / cfg.model + epsilon)

    def scaled_by(wide, which):
        return (wide * (r.gain0, r.gain1, r.gain2)[which][...]).astype(bf16)

    def start(owner):
        return owner * base + jnp.clip(owner - lo, 0, rem)

    def extra(owner):
        return jnp.logical_and(owner >= lo, owner < lo + rem)

    def gated(wide, which, gate, up, down, down_load, send, recv, sems, hid, hid_sems, fill):
        scaled = scaled_by(wide, which)
        order = far_first + [0]

        def part(owner, offset, size):
            place = lanes((start(owner) + offset) * LANE, size)
            return dot(scaled, gate[:, place]).astype(bf16), dot(scaled, up[:, place]).astype(bf16)

        def scatter(index, offset, size, begin_at):
            cut = pl.ds(begin_at, 2 * size)
            own = None
            for i in order:
                owner = kv_partner[i]
                target = send.at[owner] if i else recv.at[me_k]
                g, u = part(owner, offset, size)
                target[:, begin_at : begin_at + size] = g
                target[:, begin_at + size : begin_at + 2 * size] = u
                if i:
                    copy = pltpu.make_async_remote_copy(
                        src_ref=send.at[owner, :, cut],
                        dst_ref=recv.at[me_k, :, cut],
                        send_sem=r.send_sem.at[len(groups)],
                        recv_sem=sems.at[index],
                        device_id=(owner, me_t),
                        device_id_type=MESH,
                    )
                    when(extra(owner) if index else None, copy.start)
            own = r.send_sem.at[len(groups)]
            groups.append(n - 1)
            if index == 0:
                sent(own, send.at[pl.ds(0, n - 1), :, cut])
            else:
                mine = extra(me_k)
                if rem > 1:
                    sent(own, send.at[pl.ds(0, rem - 1), :, cut], mine)
                sent(own, send.at[pl.ds(0, rem), :, cut], jnp.logical_not(mine))

        if base:
            scatter(0, 0, main, 0)
        send_squares(wide, which)
        if rem:
            scatter(1, base, LANE, 2 * main)
        fill()
        inv = inverse(which)

        def activate(index, begin_at, size):
            cut = slice(begin_at, begin_at + 2 * size)
            arrive(recv.at[pl.ds(0, n - 1), :, pl.ds(begin_at, 2 * size)], sems.at[index])
            total = recv[0, :, cut].astype(f32)
            for source in range(1, n):
                total += recv[source, :, cut].astype(f32)
            a = total[:, :size] * inv
            b = total[:, size:] * inv
            return (a * (1.0 / (1.0 + jnp.exp(-a))) * b).astype(bf16)

        my_main = lanes(start(me_k) * LANE, main) if base else None
        my_extra = lanes((start(me_k) + base) * LANE, LANE)
        mine = extra(me_k)
        half_tiles = (n // 2) * base + min(max(n // 2 - lo, 0), rem)
        halves = halved and n > 1 and half_tiles * 2 == tiles

        def hid_sem(i):
            return hid_sems.at[1 if halves and i >= n // 2 else 0]

        def hid_ship(place, size, condition):
            own = r.send_sem.at[len(groups)]
            groups.append(n - 1)
            for i in far_first:
                copy = pltpu.make_async_remote_copy(
                    src_ref=hid.at[:, place],
                    dst_ref=hid.at[:, place],
                    send_sem=own,
                    recv_sem=hid_sem(i),
                    device_id=(kv_partner[i], me_t),
                    device_id_type=MESH,
                )
                when(condition, copy.start)
            sent(own, send.at[pl.ds(0, n - 1), :, pl.ds(0, size)], condition)

        if base:
            hid[:, my_main] = activate(0, 0, main)
            hid_ship(my_main, main, None)
        if rem:

            def do_extra():
                hid[:, my_extra] = activate(1, 2 * main, LANE)

            pl.when(mine)(do_extra)
            hid_ship(my_extra, LANE, mine)
        finish(down_load)

        def hid_arrive(index, all_tiles, with_me):
            if not with_me:
                arrive(hid.at[:, pl.ds(0, all_tiles * LANE)], hid_sems.at[index])
                return

            def wait_for(count):
                def wait():
                    arrive(hid.at[:, pl.ds(0, count * LANE)], hid_sems.at[index])

                return wait

            if rem and all_tiles > base + 1:
                pl.when(mine)(wait_for(all_tiles - base - 1))
            if all_tiles > base:
                when(jnp.logical_not(mine) if rem else None, wait_for(all_tiles - base))

        if halves:
            size = half_tiles * LANE
            near = jnp.where(me_k < n // 2, 0, size)
            hid_arrive(0, half_tiles, True)
            total = dot(hid[:, lanes(near, size)], down[lanes(near, size), :])
            hid_arrive(1, half_tiles, False)
            far = size - near
            return total + dot(hid[:, lanes(far, size)], down[lanes(far, size), :])
        hid_arrive(0, tiles, True)
        size = tiles * LANE
        return dot(hid[:, :size], down[...])

    def tp_total(part, buffer, sems):
        buffer[me_t] = part.astype(bf16)
        tp_broadcast(buffer, sems)
        tp_await(buffer, sems)
        total = buffer[0].astype(f32)
        for source in range(1, t):
            total += buffer[source].astype(f32)
        return total

    if gather_here:
        tok_all = r.tok_all
        tp_broadcast(tok_all, r.tok_sem.at[0])
    if staged:
        greet(r.greet_sem.at[0], adjacent)
    begin(loads.d1, loads.wq, loads.wk, loads.wv, loads.vc, loads.wo, loads.g2, loads.u2, loads.d2)
    if staged:
        pl.semaphore_wait(r.greet_sem.at[0], count(adjacent))
        greet(r.greet_sem.at[1], within)
    for ref in (r.g1, r.u1):
        if ref.shape[1] > units:
            ref[:, units:] = jnp.zeros((ref.shape[0], ref.shape[1] - units), bf16)
    finish(loads.g1, loads.u1, *small)
    if staged:
        pl.semaphore_wait(r.greet_sem.at[1], count(within))
    if gather_here:
        tp_await(tok_all, r.tok_sem.at[0])
        wide = jnp.concatenate([tok_all[s].astype(f32) for s in range(t)], axis=1)
    else:
        wide = r.tok_in[...].astype(f32)

    def nothing():
        pass

    def turn_keys(lower, upper):
        kc, kt = r.kc, r.kt

        def one(b, carry):
            kt[b] = kc[b].T
            return carry

        lax.fori_loop(lower, upper, one, 0, unroll=2)

    def first_fill():
        flat = positions * heads
        row_head = lax.rem(lax.broadcasted_iota(jnp.int32, (2 * heads, flat), 0), heads)
        column = lax.broadcasted_iota(jnp.int32, (2 * heads, flat), 1)
        r.pos[...] = jnp.where(
            lax.rem(column, heads) == row_head,
            column // heads + me_k * positions,
            jnp.int32(2**30),
        )
        pick_row = lax.broadcasted_iota(jnp.int32, (LANE, 4 * LANE), 0)
        pick_block = lax.broadcasted_iota(jnp.int32, (LANE, 4 * LANE), 1) // LANE
        r.pick[...] = jnp.where(pick_row // 3 == pick_block, 1.0, 0.0).astype(bf16)

        if cfg.turned:
            finish(loads.kc)
            turn_keys(0, rows)
        for ref in (r.g2, r.u2):
            if ref.shape[1] > units:
                ref[:, units:] = jnp.zeros((ref.shape[0], ref.shape[1] - units), bf16)
        for ref in (r.d1, r.d2):
            if ref.shape[0] > units:
                ref[units:, :] = jnp.zeros((ref.shape[0] - units, ref.shape[1]), bf16)

    part = gated(
        wide,
        0,
        r.g1,
        r.u1,
        r.d1,
        loads.d1,
        r.gu_send1,
        r.gu_recv1,
        r.gu_sem1,
        r.hid1,
        r.hid_sem1,
        first_fill,
    )
    first = (wide + 0.5 * tp_total(part, r.down1, r.down_sem1.at[0])).astype(bf16).astype(f32)

    finish(loads.wq)
    scaled = scaled_by(first, 1)
    q_send, q_recv, q_sem = r.q_send, r.q_recv, r.q_sem
    halves = 2 if heads % 2 == 0 else 1
    half_inner = inner // halves
    for side in range(halves):
        cut = pl.ds(side * half_inner, half_inner)
        query_part = dot(scaled, r.wq[:, cut]).astype(bf16)
        for c in range(chunks):
            q_send[c, :, cut] = query_part[c * chunk : (c + 1) * chunk]
        if side < halves - 1:
            starts = [
                (q_send.at[0, :, cut], q_recv.at[me_k, 0, :, cut], kv_partner[i], None)
                for i in far_first
            ]
            ship(starts, q_sem.at[0], "kv", len(groups))
    for c in range(chunks):
        cut = pl.ds((halves - 1) * half_inner, half_inner) if c == 0 else pl.ds(0, inner)
        own = ship(
            [
                (q_send.at[c, :, cut], q_recv.at[me_k, c, :, cut], kv_partner[i], None)
                for i in far_first
            ],
            q_sem.at[c],
            "kv",
        )
        sent(own, q_recv.at[pl.ds(0, n - 1), c])
        if c == 0:
            send_squares(first, 1)

    kv_send, kv_recv, kv_sem = r.kv_send, r.kv_recv, r.kv_sem
    finish(loads.wk, loads.wv)
    key_part = dot(scaled, r.wk[...]).astype(bf16)
    value_part = dot(scaled, r.wv[...]).astype(bf16)
    shift = jnp.where(me_k < n // 2, owners // 2, 0)
    my_place = me_k - first_owner
    is_owner = jnp.logical_and(my_place >= 0, my_place < owners)
    my_slot = jnp.clip(my_place, 0, owners - 1)
    for j in range(owners):
        kv_send[j, :, :share] = key_part[:, j * share : (j + 1) * share]
        kv_send[j, :, share:] = value_part[:, j * share : (j + 1) * share]
    owner_order = [lax.rem(j + shift, owners) for j in range(owners)]

    def to_owners(source, target, sem):
        own = ship(
            [
                (source.at[j], target, j + first_owner, me_k != j + first_owner)
                for j in owner_order
            ],
            sem,
            "kv",
        )
        if owners > 1:
            sent(own, source.at[pl.ds(0, owners - 1)], is_owner)
        sent(own, source.at[pl.ds(0, owners)], jnp.logical_not(is_owner))

    to_owners(kv_send, kv_recv.at[me_k], kv_sem.at[0])

    inv = inverse(1)
    logit_scale = HEAD_DIM ** (-0.5)
    wide_lane = lax.broadcasted_iota(jnp.int32, (2 * heads, LANE), 1)
    third = lax.rem(wide_lane, 3)
    map_row = lax.broadcasted_iota(jnp.int32, (2 * heads, LANE), 0) // heads
    slot = wide_lane - 6 * map_row
    first_half = lax.broadcasted_iota(jnp.int32, (chunk, LANE), 1) < HEAD_DIM
    finish(loads.vc)
    if not cfg.turned:
        finish(loads.kc)
    kc, vc, kt, qf, acc, q_all = r.kc, r.vc, r.kt, r.qf, r.acc, r.q_all
    score_ref, pos, lengths = r.score, r.pos, r.lengths
    att_send, att_recv, part_sem = r.att_send, r.att_recv, r.part_sem

    def attend(c):
        q_recv[me_k, c] = q_send[c]
        arrive(q_recv.at[pl.ds(0, n - 1), c], q_sem.at[c])
        total = q_recv[0, c].astype(f32)
        for source in range(1, n):
            total += q_recv[source, c].astype(f32)
        query = (total * inv[c * chunk : (c + 1) * chunk]).astype(bf16)
        q_all[c * chunk : (c + 1) * chunk, :] = query.astype(f32)
        for h in range(heads):
            block = query[:, h * VAL_DIM : (h + 1) * VAL_DIM].astype(f32) * logit_scale
            qf[:, h, :] = jnp.where(first_half, block, 0.0)
            qf[:, heads + h, :] = jnp.where(first_half, 0.0, block)
        for i in range(chunk):
            b = c * chunk + i
            if cfg.turned:
                score_ref[i] = dot(qf[i].astype(bf16), kt[b])
            else:
                score_ref[i] = lax.dot_general(
                    qf[i].astype(bf16),
                    kc[b],
                    (((1,), (1,)), ((), ())),
                    preferred_element_type=f32,
                )
        for i in range(chunk):
            b = c * chunk + i
            score = jnp.where(pos[...] < lengths[b], score_ref[i], neg_fill)
            peak = jnp.max(score, axis=1, keepdims=True)
            weight = jnp.exp(score - peak)
            mass = jnp.sum(weight, axis=1, keepdims=True)
            acc[i, :, :LANE] = dot(weight.astype(bf16), vc[b])
            stats = jnp.where(
                slot < 0, 0.0, jnp.where(slot < 3, peak, jnp.where(slot < 6, mass, 0.0))
            )
            high = stats.astype(bf16).astype(f32)
            mid = (stats - high).astype(bf16).astype(f32)
            low = stats - high - mid
            acc[i, :, LANE:] = jnp.where(third == 0, high, jnp.where(third == 1, mid, low))
        for j in range(owners):
            for p in range(per):
                head = j * per + p
                one, two = acc[:, head, :], acc[:, heads + head, :]
                place = pl.ds(p * chunk, chunk)
                att_send[c, j, place, :LANE] = one[:, :LANE].astype(bf16)
                att_send[c, j, place, LANE : 2 * LANE] = two[:, :LANE].astype(bf16)
                att_send[c, j, place, 2 * LANE :] = (one[:, LANE:] + two[:, LANE:]).astype(bf16)
        to_owners(att_send.at[c], att_recv.at[me_k, c], part_sem.at[c])

    for c in range(chunks):
        attend(c)

    att_all, att_sem = r.att_all, r.att_sem
    my_share = lanes(my_slot * share, share)
    half = lax.broadcasted_iota(jnp.int32, (per * chunk, LANE), 1) < HEAD_DIM

    def combine():
        kv_recv[me_k] = kv_send[my_slot]
        arrive(kv_recv.at[pl.ds(0, n - 1)], kv_sem.at[0])
        fresh = kv_recv[0].astype(f32)
        for source in range(1, n):
            fresh += kv_recv[source].astype(f32)
        fresh = (fresh * inv).astype(bf16).astype(f32)
        fresh_key, fresh_value = fresh[:, :share], fresh[:, share:]
        query = q_all[:, my_share]
        product = query * fresh_key * logit_scale

        def stacked(x, c):
            return jnp.concatenate(
                [
                    x[c * chunk : (c + 1) * chunk, p * VAL_DIM : (p + 1) * VAL_DIM]
                    for p in range(per)
                ],
                axis=0,
            )

        own = []
        for c in range(chunks):
            block = stacked(product, c)
            own.append(
                [
                    jnp.sum(jnp.where(half, block, 0.0), axis=1, keepdims=True),
                    jnp.sum(jnp.where(half, 0.0, block), axis=1, keepdims=True),
                ]
            )
        lam_rows = jnp.concatenate(
            [jnp.full((chunk, LANE), r.lam[my_slot * per + p], f32) for p in range(per)], axis=0
        )
        for c in range(chunks):
            att_recv[me_k, c] = att_send[c, my_slot]
            arrive(att_recv.at[pl.ds(0, n - 1), c], part_sem.at[c])
            stats = jnp.concatenate(
                [att_recv[source, c, :, 2 * LANE :] for source in range(n)], axis=0
            )
            stats = dot(stats, r.pick[...])
            high = per * chunk
            new_value = stacked(fresh_value, c)
            maps = []
            for m in range(2):
                peaks = [
                    stats[s * high : (s + 1) * high, 2 * m * LANE : (2 * m + 1) * LANE]
                    for s in range(n)
                ]
                masses = [
                    stats[s * high : (s + 1) * high, (2 * m + 1) * LANE : (2 * m + 2) * LANE]
                    for s in range(n)
                ]
                highest = jnp.broadcast_to(own[c][m], (high, LANE))
                for peak in peaks:
                    highest = jnp.maximum(highest, peak)
                own_weight = jnp.exp(own[c][m] - highest)
                den = own_weight
                num = own_weight.astype(bf16).astype(f32) * new_value
                for source in range(n):
                    scale = jnp.exp(peaks[source] - highest)
                    den += scale * masses[source]
                    num += scale * att_recv[source, c, :, m * LANE : (m + 1) * LANE].astype(f32)
                maps.append(num / den)
            mixed = maps[0] - lam_rows * maps[1]
            normed = (
                mixed
                * lax.rsqrt(jnp.mean(mixed * mixed, axis=1, keepdims=True) + epsilon)
                * r.head_gain[...]
            )
            for p in range(per):
                r.att_own[c * chunk : (c + 1) * chunk, p * VAL_DIM : (p + 1) * VAL_DIM] = (
                    normed[p * chunk : (p + 1) * chunk]
                )
        att_all[:, my_share] = r.att_own[...].astype(bf16)

    pl.when(is_owner)(combine)
    att_halves = halved and owners % 2 == 0 and 2 * first_owner + owners == n
    own = r.send_sem.at[len(groups)]
    groups.append(n - 1)
    for i in far_first:
        copy = pltpu.make_async_remote_copy(
            src_ref=att_all.at[:, my_share],
            dst_ref=att_all.at[:, my_share],
            send_sem=own,
            recv_sem=att_sem.at[1 if att_halves and i >= n // 2 else 0],
            device_id=(kv_partner[i], me_t),
            device_id_type=MESH,
        )
        when(is_owner, copy.start)
    sent(own, kv_recv.at[pl.ds(0, n - 1), :, pl.ds(0, share)], is_owner)
    finish(loads.wo)

    def att_arrive(index, count):
        if count:
            arrive(att_all.at[:, pl.ds(0, count * share)], att_sem.at[index])

    def att_arrive_near(count):
        pl.when(is_owner)(lambda: att_arrive(0, count - 1))
        pl.when(jnp.logical_not(is_owner))(lambda: att_arrive(0, count))

    wo = r.wo
    if att_halves:
        size = owners // 2 * share
        near = jnp.where(me_k < n // 2, 0, size)
        att_arrive_near(owners // 2)
        part = dot(att_all[:, lanes(near, size)], wo[lanes(near, size), :])
        att_arrive(1, owners // 2)
        far = size - near
        part += dot(att_all[:, lanes(far, size)], wo[lanes(far, size), :])
    else:
        att_arrive_near(owners)
        part = dot(att_all[...], wo[...])
    second = (first + tp_total(part, r.out_all, r.out_sem.at[0])).astype(bf16).astype(f32)

    finish(loads.g2, loads.u2)
    stream, result = r.stream, r.result
    stream[...] = second
    part = gated(
        second,
        2,
        r.g2,
        r.u2,
        r.d2,
        loads.d2,
        r.gu_send2,
        r.gu_recv2,
        r.gu_sem2,
        r.hid2,
        r.hid_sem2,
        nothing,
    )
    if gather_here:
        down2, down2_recv, sem = r.down2, r.down2_recv, r.down_sem2.at[0]
        for s in range(t):
            down2[s] = part[:, s * cols : (s + 1) * cols].astype(bf16)
        own = ship(
            [(down2.at[peer], down2_recv.at[me_t], peer, None) for peer in tp_partner[:0:-1]],
            sem,
            "tp",
        )
        sent(own, down2.at[pl.ds(0, t - 1)])
        down2_recv[me_t] = down2[me_t]
        tp_await(down2_recv, sem)
        total = down2_recv[0].astype(f32)
        for source in range(1, t):
            total += down2_recv[source].astype(f32)
        own = stream[:, lanes(me_t * cols, cols)]
        result[...] = (own + 0.5 * total).astype(bf16)
    else:
        total = tp_total(part, r.down2, r.down_sem2.at[0])
        result[...] = (second + 0.5 * total).astype(bf16)
    for copy, condition in sends:
        when(condition, copy.wait_send)


def on_device(
    tokens,
    first_gain,
    first_gate,
    first_up,
    first_down,
    mixer_gain,
    w_query,
    w_key,
    w_value,
    w_output,
    lam_heads,
    head_gain,
    key_cache,
    value_cache,
    lengths,
    last_gain,
    last_gate,
    last_up,
    last_down,
):
    n, t = lax.axis_size("kv"), lax.axis_size("tp")
    rows, cols = tokens.shape
    width, units = first_gate.shape
    positions, heads = key_cache.shape[1:3]
    gather_here = cols % LANE == 0
    tiles = ceil_div(units, LANE)
    base, rem = divmod(tiles, n)
    lo = (n - rem) // 2
    owners = heads // 2 if heads % 2 == 0 and heads // 2 <= n else heads
    per = heads // owners
    chunks = 2 if rows % 16 == 0 else 1
    chunk = rows // chunks
    inner = heads * VAL_DIM
    share = per * VAL_DIM
    cfg = types.SimpleNamespace(
        n=n,
        t=t,
        model=width * n,
        rows=rows,
        cols=cols,
        units=units,
        heads=heads,
        positions=positions,
        tiles=tiles,
        base=base,
        rem=rem,
        lo=lo,
        owners=owners,
        per=per,
        first_owner=(n - owners) // 2,
        gather_here=gather_here,
        chunks=chunks,
        chunk=chunk,
        turned=TURNED,
    )
    if not gather_here:
        tokens = lax.all_gather(tokens, "tp", axis=1, tiled=True)
    flat = positions * heads
    keys = key_cache.reshape(rows, flat, VAL_DIM)
    values = value_cache.reshape(rows, flat, VAL_DIM)

    wide_units = (tiles + (1 if rem else 0)) * LANE
    gu = (n, rows, 2 * (base + (1 if rem else 0)) * LANE)
    dma = pltpu.SemaphoreType.DMA
    return_cols = cols if gather_here else width
    inputs = dict(
        tokens=tokens,
        gain0_in=first_gain.reshape(1, width),
        gain1_in=mixer_gain.reshape(1, width),
        gain2_in=last_gain.reshape(1, width),
        head_gain_in=head_gain.reshape(1, VAL_DIM),
        lam_in=lam_heads,
        lengths_in=lengths,
        first_gate=first_gate,
        first_up=first_up,
        first_down=first_down,
        w_query=w_query,
        w_key=w_key,
        w_value=w_value,
        w_output=w_output,
        keys=keys,
        values=values,
        last_gate=last_gate,
        last_up=last_up,
        last_down=last_down,
    )
    scratch = dict(
        gain0=((1, width), f32),
        gain1=((1, width), f32),
        gain2=((1, width), f32),
        head_gain=((1, VAL_DIM), f32),
        g1=((width, wide_units), bf16),
        u1=((width, wide_units), bf16),
        d1=((tiles * LANE, width), bf16),
        wq=((width, inner), bf16),
        wk=((width, inner), bf16),
        wv=((width, inner), bf16),
        wo=((inner, width), bf16),
        kc=((rows, flat, VAL_DIM), bf16),
        vc=((rows, flat, VAL_DIM), bf16),
        kt=((rows, VAL_DIM, flat) if TURNED else (1, VAL_DIM, LANE), bf16),
        g2=((width, wide_units), bf16),
        u2=((width, wide_units), bf16),
        d2=((tiles * LANE, width), bf16),
        stream=((rows, width), f32),
        squares=((3, n, 1, LANE), f32),
        gu_send1=(gu, bf16),
        gu_recv1=(gu, bf16),
        gu_send2=(gu, bf16),
        gu_recv2=(gu, bf16),
        hid1=((rows, wide_units), bf16),
        hid2=((rows, wide_units), bf16),
        down1=((t, rows, width), bf16),
        out_all=((t, rows, width), bf16),
        q_send=((chunks, chunk, inner), bf16),
        q_recv=((n, chunks, chunk, inner), bf16),
        q_all=((rows, inner), f32),
        kv_send=((owners, rows, 2 * share), bf16),
        kv_recv=((n, rows, 2 * share), bf16),
        qf=((chunk, 2 * heads, VAL_DIM), f32),
        score=((chunk, 2 * heads, flat), f32),
        acc=((chunk, 2 * heads, VAL_DIM + LANE), f32),
        pos=((2 * heads, flat), jnp.int32),
        pick=((LANE, 4 * LANE), bf16),
        att_send=((chunks, owners, per * chunk, 2 * VAL_DIM + LANE), bf16),
        att_recv=((n, chunks, per * chunk, 2 * VAL_DIM + LANE), bf16),
        att_own=((rows, share), f32),
        att_all=((rows, inner), bf16),
    )
    if gather_here:
        scratch.update(
            tok_all=((t, rows, cols), bf16),
            down2=((t, rows, cols), bf16),
            down2_recv=((t, rows, cols), bf16),
        )
    else:
        scratch.update(tok_in=((rows, width), bf16), down2=((t, rows, width), bf16))
    sems = dict(
        load_sem=(19,),
        send_sem=(3 + 8 + 2 * chunks + 2 + 4,),
        tok_sem=(1,),
        sq_sem=(3,),
        gu_sem1=(2,),
        gu_sem2=(2,),
        hid_sem1=(2,),
        hid_sem2=(2,),
        down_sem1=(1,),
        down_sem2=(1,),
        out_sem=(1,),
        q_sem=(chunks,),
        kv_sem=(1,),
        part_sem=(chunks,),
        att_sem=(2,),
    )
    smem = dict(lam=(lam_heads.shape, f32), lengths=(lengths.shape, jnp.int32))
    names = [*inputs, *dict(result=0), *scratch, *smem, *sems, *dict(greet_sem=0)]
    result = pl.pallas_call(
        functools.partial(layer_kernel, cfg, names),
        out_shape=pltpu.VMEM((rows, return_cols), bf16),
        in_specs=[pl.BlockSpec(memory_space=pl.ANY)] * len(inputs),
        out_specs=pl.BlockSpec(memory_space=pltpu.VMEM),
        scratch_shapes=[pltpu.VMEM(shape, kind) for shape, kind in scratch.values()]
        + [pltpu.SMEM(shape, kind) for shape, kind in smem.values()]
        + [dma(shape) for shape in sems.values()]
        + [pltpu.SemaphoreType.REGULAR((2,))],
        compiler_params=pltpu.CompilerParams(
            collective_id=0, has_side_effects=True, vmem_limit_bytes=63 * 2**20
        ),
    )(*inputs.values())
    if not gather_here:
        result = lax.dynamic_slice_in_dim(result, lax.axis_index("tp") * cols, cols, 1)
    return result


TURNED = True


def solution(mesh):
    return jax.shard_map(
        on_device,
        mesh=mesh,
        in_specs=(
            P(None, ("kv", "tp")),
            P("kv"),
            P("kv", "tp"),
            P("kv", "tp"),
            P("tp", "kv"),
            P("kv"),
            P("kv", "tp"),
            P("kv", "tp"),
            P("kv", "tp"),
            P("tp", "kv"),
            P("tp"),
            P(),
            P(None, "kv", "tp", None),
            P(None, "kv", "tp", None),
            P(),
            P("kv"),
            P("kv", "tp"),
            P("kv", "tp"),
            P("tp", "kv"),
        ),
        out_specs=P(None, ("kv", "tp")),
        check_vma=False,
    )
```

time: 60.3 us -> 57.2 us (0.949)
  Pallas kernels: 59.5 us -> 56.5 us
    pallas_call x1, Pallas kernels: 59.5 us -> 56.5 us  [on_device(): pl.pallas_call(functools.partial(layer_kernel, cfg, names), out_shape=plt...]
where the time goes in v2:
time: 57.2 us; the launch traced here: 57.1 us
  Pallas kernels  56.5 us (99%)
  local copies, waits for them, and re-layouts  0.6 us (1%)
    pallas_call x1, Pallas kernels, on_device(): pl.pallas_call(functools.partial(layer_kernel, cfg, names), out_shape=plt...  56.5 us

profile of v2, /device:TPU:0, one launch (start us, length us, event | category | flops | bytes accessed | tf_op | source)
XLA Modules:
  0.0 57.1 jit_solution(14699833847958862909)
XLA Ops:
  0.0 56.5 %shard_map.181 = bf16[16,128]{1,0:T(8,128)(2,1)S(1)} custom-call(bf16[16,128]{1,0:T(8,128)(2,1)} %refs_0_.1, f32[1,512]{1,0:T(1,128)} %bitcast.8, f32[1,512]{1,0:T(1,128)} %bitcast.9, f32[1,512]{1,0:T(1,128)} %bitcast.10, f32[1,128]{1,0:T(1,128)} %bitcast.11, f32[8]{0:T(128)} %refs_5_.1, s32[16]{0:T(128)} %refs_6_.1, bf16[512,2816]{1,0:T(8,128)(2,1)} %refs_7_.1, ...), custom_call_target="tpu_custom_call" | custom-call | tf_op jit(solution)/shard_map/pallas_call | solution.py:872
  56.5 0.6 %copy.21 = bf16[16,128]{1,0:T(8,128)(2,1)} copy(bf16[16,128]{1,0:T(8,128)(2,1)S(1)} %shard_map.181) | data formatting | bytes 8192
